TPU v7x, 32 devices: a whole 2x2x4 slice. The times are simulated.
32 devices in a mesh: grp: 2 (over y), sp: 8 (over z, core), tp: 2 (over x).
Axes of the slice: x: 2, y: 2, z: 4, core: 2. Of those that a mesh axis runs over, the one named last changes fastest.
Arguments:
- query_plain: bfloat16 [2560, 1024], P(('grp', 'sp'), 'tp'), parts along dimension 0, may hold values from -6 to 6
- query_turn: bfloat16 [2560, 512], P(('grp', 'sp'), 'tp'), parts along dimension 0, may hold values from -40 to 40, as said below
- latent: bfloat16 [2560, 512], P(('grp', 'sp')), parts along dimension 0, may hold values from -6 to 6
- key_turn: bfloat16 [2560, 64], P(('grp', 'sp')), parts along dimension 0, may hold values from -40 to 40, as said below
- latent_norm_scale: bfloat16 [512], replicated, may hold values from 0.099609375 to 1.8984375
- plain_key_matrix: bfloat16 [512, 1024], P(None, 'tp'), may hold values from -0.25 to 0.25
- value_matrix: bfloat16 [512, 1024], P(None, 'tp'), may hold values from -0.25 to 0.25
- residual: bfloat16 [2560, 2048], P(('grp', 'sp', 'tp')), parts along dimension 0, may hold values from -6 to 6
- out_weight: bfloat16 [1024, 2048], replicated, may hold values from -6 to 6
- ffn_gain: bfloat16 [2048], replicated, may hold values from 0.099609375 to 1.8984375
- gate_weight: bfloat16 [8, 2048, 1024], P('sp', None, 'tp'), may hold values from -1 to 1
- up_weight: bfloat16 [8, 2048, 1024], P('sp', None, 'tp'), may hold values from -1 to 1
- down_weight: bfloat16 [8, 1024, 2048], P('sp', 'tp'), may hold values from -0.0625 to 0.0625
- routes: int32 [2560, 4], P(('grp', 'sp', 'tp')), parts along dimension 0, may hold values from 0 to 7, all different within a row; in each aligned block of 80 rows (0 to 79, 80 to 159, ...) at most 60 rows name the same one
- route_weights: float32 [2560, 4], P(('grp', 'sp', 'tp')), parts along dimension 0, may hold values from 0.1 to 0.6
Outputs:
- mixed: bfloat16 [2560, 2048], P(('grp', 'sp', 'tp')), parts along dimension 0
There are 2 independent parts, one for each index of `grp`. A program takes and returns all parts, laid end to end along the dimension named above; an argument that names none is the same for every part. Nothing has to cross between parts.
Inputs may be any that keep to these rules, and one draw needn't show every extreme that they name: `query_turn`: in the hidden draw some rows are large. `key_turn`: in the hidden draw some rows are large. `routes`: each row names 4 different experts. In each aligned block of 80 rows (the rows of one device) no expert is named more than 60 times, a bound that some block reaches.
All inputs are finite; a program needn't handle non-finite values.
Results may differ from a plain program's by a relative error of at most 0.015.
Values may be sent and summed in bfloat16 or wider, within the bound.
A program may use at most 128 MiB of HBM per device.

v0:
```python
import jax
import jax.numpy as jnp
from jax import lax
from jax.sharding import PartitionSpec as P

PLAIN_HEAD_WIDTH = 128
QK_ROPE = 64
VALUE_WIDTH = 128
GRID_W = 64
theta = 10000.0
eps = 1e-06
limit = 7.0
slope = 1.702


def turn(vector, row_shift, col_shift):
    width = vector.shape[-1]
    count = width // 4
    half = width // 2
    freqs = theta ** (-jnp.arange(count, dtype=jnp.float32) / count)
    extra = (1,) * (vector.ndim - 2)
    pieces = []
    for portion, shift in ((vector[..., :half], row_shift), (vector[..., half:], col_shift)):
        angle = (shift.astype(jnp.float32)[:, None] * freqs[None, :]).reshape(
            (shift.shape[0],) + extra + (count,)
        )
        lower = portion[..., :count]
        upper = portion[..., count:]
        pieces.append(
            jnp.concatenate(
                [
                    lower * jnp.cos(angle) - upper * jnp.sin(angle),
                    lower * jnp.sin(angle) + upper * jnp.cos(angle),
                ],
                axis=-1,
            )
        )
    return jnp.concatenate(pieces, axis=-1)


def norm_scale(values, gain):
    wide = values.astype(jnp.float32)
    return (
        wide
        * lax.rsqrt(jnp.mean(wide * wide, axis=-1, keepdims=True) + eps)
        * gain.astype(jnp.float32)
    )


def expert_active(rows, gate_w, up_w):
    gate_pre = jnp.minimum(jnp.dot(rows, gate_w, preferred_element_type=jnp.float32), limit)
    up_pre = jnp.clip(jnp.dot(rows, up_w, preferred_element_type=jnp.float32), -limit, limit)
    return ((up_pre + 1.0) * gate_pre * jax.nn.sigmoid(slope * gate_pre)).astype(jnp.bfloat16)


def on_device(
    query_plain,
    query_turn,
    latent,
    key_turn,
    latent_norm_scale,
    plain_key_matrix,
    value_matrix,
    residual,
    out_weight,
    ffn_gain,
    gate_weight,
    up_weight,
    down_weight,
    routes,
    route_weights,
):
    tok_dev = latent.shape[0]
    heads_dev = query_plain.shape[1] // PLAIN_HEAD_WIDTH
    model_width = residual.shape[1]
    place = lax.axis_index("sp") * tok_dev + jnp.arange(tok_dev, dtype=jnp.int32)
    grid_row = place // GRID_W
    grid_col = place % GRID_W
    normed_latent = norm_scale(latent, latent_norm_scale).astype(jnp.bfloat16)
    key_rot = turn(key_turn.astype(jnp.float32), grid_row, grid_col).astype(jnp.bfloat16)
    expert_ids = jnp.arange(lax.axis_size("sp"), dtype=jnp.int32)
    share = jnp.sum(
        route_weights[..., None] * (routes[..., None] == expert_ids).astype(jnp.float32), axis=1
    )
    latent_width = latent.shape[1]
    sent = jnp.concatenate([normed_latent, key_rot], axis=1)
    everyone = lax.all_gather(sent, "sp", axis=0, tiled=True)
    shares = lax.all_gather(share, ("sp", "tp"), axis=0, tiled=True)
    all_latent = everyone[:, :latent_width]
    all_rot = everyone[:, latent_width:]
    keys = jnp.dot(all_latent, plain_key_matrix, preferred_element_type=jnp.float32).astype(
        jnp.bfloat16
    )
    values = jnp.dot(all_latent, value_matrix, preferred_element_type=jnp.float32).astype(
        jnp.bfloat16
    )
    query_rot = turn(
        query_turn.astype(jnp.float32).reshape(tok_dev, heads_dev, QK_ROPE), grid_row, grid_col
    ).astype(jnp.bfloat16)
    scale = (PLAIN_HEAD_WIDTH + QK_ROPE) ** (-0.5)
    attended = []
    for head in range(heads_dev):
        span = slice(head * PLAIN_HEAD_WIDTH, (head + 1) * PLAIN_HEAD_WIDTH)
        scores = (
            jnp.einsum(
                "qd,kd->qk", query_plain[:, span], keys[:, span], preferred_element_type=jnp.float32
            )
            + jnp.einsum(
                "qd,kd->qk", query_rot[:, head], all_rot, preferred_element_type=jnp.float32
            )
        ) * scale
        weights = jnp.exp(scores - jnp.max(scores, axis=1, keepdims=True))
        summed = jnp.dot(
            weights.astype(jnp.bfloat16),
            values[:, head * VALUE_WIDTH : (head + 1) * VALUE_WIDTH],
            preferred_element_type=jnp.float32,
        )
        attended.append((summed / jnp.sum(weights, axis=1, keepdims=True)).astype(jnp.bfloat16))
    attended = jnp.concatenate(attended, axis=1)
    rows_dev = residual.shape[0]
    group = lax.axis_size("tp")
    swapped = lax.all_to_all(
        attended.reshape(group, rows_dev, heads_dev * VALUE_WIDTH),
        "tp",
        split_axis=0,
        concat_axis=0,
        tiled=True,
    )
    own_rows = jnp.transpose(swapped, (1, 0, 2)).reshape(rows_dev, group * heads_dev * VALUE_WIDTH)
    projected = jnp.dot(own_rows, out_weight, preferred_element_type=jnp.float32)
    hidden = (residual.astype(jnp.float32) + projected).astype(jnp.bfloat16)
    normed = norm_scale(hidden, ffn_gain).astype(jnp.bfloat16)
    rows = lax.all_gather(normed, ("sp", "tp"), axis=0, tiled=True)
    active = expert_active(rows, gate_weight[0], up_weight[0])
    product = jnp.dot(active, down_weight[0], preferred_element_type=jnp.float32)
    own_share = jnp.sum(
        jnp.where(expert_ids[None, :] == lax.axis_index("sp"), shares, 0.0), axis=1, keepdims=True
    )
    mixture = lax.psum_scatter(
        (own_share * product).astype(jnp.bfloat16), ("sp", "tp"), scatter_dimension=0, tiled=True
    )
    return (hidden.astype(jnp.float32) + mixture.astype(jnp.float32)).astype(jnp.bfloat16)


def solution(mesh):
    placed = (
        P(("grp", "sp"), "tp"),
        P(("grp", "sp"), "tp"),
        P(("grp", "sp"), None),
        P(("grp", "sp"), None),
        P(),
        P(None, "tp"),
        P(None, "tp"),
        P(("grp", "sp", "tp"), None),
        P(),
        P(),
        P("sp", None, "tp"),
        P("sp", None, "tp"),
        P("sp", "tp", None),
        P(("grp", "sp", "tp"), None),
        P(("grp", "sp", "tp"), None),
    )
    return jax.shard_map(
        on_device,
        mesh=mesh,
        in_specs=placed,
        out_specs=P(("grp", "sp", "tp"), None),
        check_vma=False,
    )
```

profile of v0, /device:TPU:0, one launch (start us, length us, event | category | flops | bytes accessed | tf_op | source)
XLA Modules:
  0.0 219.9 jit_solution(17451108675109857187)
XLA Ops:
  6.6 1.2 fusion.37
  7.8 0.7 convert_element_type.92
  8.5 0.8 convert_element_type.94
  9.2 0.2 multiply_cosine_fusion
  9.5 0.1 copy.52
  9.6 0.1 copy.51
  9.7 0.1 copy.53
  9.8 0.1 copy.54
  9.9 1.0 fusion.39
  11.0 0.8 concatenate.13
  11.8 0.0 all-gather.4.cloned.1.call-update
  11.8 1.0 copy.55
  12.9 27.4 %all-gather.4.cloned.1.call-done = bf16[1280,576]{1,0:T(8,128)(2,1)} async-done(((bf16[160,576]{1,0:T(8,128)(2,1)}), bf16[1280,576]{1,0:T(8,128)(2,1)}) %all-gather.4.cloned.1.call-update) | async-done | bytes 1474576 | tf_op jit(solution)/shard_map/all_gather | solution.py:87
  40.3 2.2 convolution_convert_fusion.1
  42.5 0.3 convolution_bitcast_fusion
  42.8 0.3 convolution_bitcast_fusion.1
  43.1 0.3 convolution_bitcast_fusion.2
  43.3 0.3 convolution_bitcast_fusion.3
  43.6 0.3 copy-done.1
  43.9 0.4 fusion.63
  44.3 0.3 fusion.27
  44.6 0.8 convolution_convert_fusion
  45.5 0.3 fusion.18
  45.8 0.4 fusion.64
  46.2 0.3 fusion.25
  46.5 0.3 fusion.17
  46.8 0.4 fusion.66
  47.2 0.3 fusion.21
  47.5 0.3 fusion.15
  47.9 0.4 fusion.65
  48.3 0.3 fusion.23
  48.6 0.3 fusion.16
  48.9 0.7 pad_maximum_fusion
  49.6 3.4 %all-to-all-start = ((bf16[2,80,512]{2,1,0:T(8,128)(2,1)}), bf16[2,80,512]{2,1,0:T(8,128)(2,1)S(1)}, u32[]{:S(2)}, u32[]{:S(2)}) async-start(bf16[2,80,512]{2,1,0:T(8,128)(2,1)} %bitcast.10), calls=%async_computation | async-start | bytes 327680 | tf_op jit(solution)/shard_map/all_to_all | solution.py:122
  53.0 0.0 all-gather.6.cloned.1.call-start
  53.1 4.7 %all-to-all-done = bf16[2,80,512]{2,1,0:T(8,128)(2,1)S(1)} async-done(((bf16[2,80,512]{2,1,0:T(8,128)(2,1)}), bf16[2,80,512]{2,1,0:T(8,128)(2,1)S(1)}, u32[]{:S(2)}, u32[]{:S(2)}) %all-to-all-start) | async-done | bytes 163872 | tf_op jit(solution)/shard_map/all_to_all | solution.py:122
  57.8 3.2 %multiply_reduce_fusion = (f32[80]{0:T(128)S(1)}, f32[80,2048]{1,0:T(8,128)S(1)}) fusion(bf16[80,1024]{1,0:T(8,128)(2,1)S(1)} %bitcast.54, bf16[1024,2048]{1,0:T(8,128)(2,1)} %param.23, bf16[80,2048]{1,0:T(8,128)(2,1)S(1)} %copy-done.2), kind=kOutput, calls=%fused_computation.51 | convolution fusion | flops 336527296 | bytes 5341504 | tf_op jit(solution)/shard_map/dot_general | solution.py:130
  61.0 0.9 multiply_convert_fusion.1
  61.9 0.0 all-gather.6.cloned.1.call-update
  61.9 0.0 reduce-scatter.2.cloned.1.call-start
  62.0 29.8 %all-gather = f32[16,80,8]{1,2,0:T(8,128)S(1)} all-gather(f32[1,80,8]{1,2,0:T(8,128)S(1)} %bitcast.57), channel_id=1, replica_groups=mesh['grp'=2,'sp'=8,'tp'=2] {'sp','tp'}, dimensions={0}, use_global_device_ids=true | all-gather | bytes 43520 | tf_op jit(solution)/shard_map/all_gather | solution.py:88
  91.8 0.1 reshape.193
  91.9 0.1 select_reduce_fusion
  92.0 24.3 %all-gather.6.cloned.1.call-done = bf16[1280,2048]{1,0:T(8,128)(2,1)} async-done(((bf16[80,2048]{1,0:T(8,128)(2,1)}), bf16[1280,2048]{1,0:T(8,128)(2,1)}) %all-gather.6.cloned.1.call-update) | async-done | bytes 5242896 | tf_op jit(solution)/shard_map/all_gather | solution.py:133
  116.4 7.6 %convolution_minimum_fusion = f32[1280,512]{1,0:T(8,128)} fusion(bf16[1280,2048]{1,0:T(8,128)(2,1)} %all-gather.6.cloned.1.call-done, bf16[1,2048,512]{2,1,0:T(8,128)(2,1)} %param.25), kind=kOutput, calls=%fused_computation.2 | convolution fusion | flops 2685009920 | bytes 9961472 | tf_op jit(solution)/shard_map/dot_general | solution.py:51
  123.9 10.5 %multiply_convert_fusion = bf16[1280,2048]{1,0:T(8,128)(2,1)} fusion(f32[1280]{0:T(1024)S(1)} %select_reduce_fusion, bf16[1,512,2048]{2,1,0:T(8,128)(2,1)S(1)} %copy-done, f32[1280,512]{1,0:T(8,128)} %convolution_minimum_fusion, bf16[1280,2048]{1,0:T(8,128)(2,1)} %all-gather.6.cloned.1.call-done, bf16[1,2048,512]{2,1,0:T(8,128)(2,1)} %param.26), kind=kOutput, calls=%fused_computation | convolution fusion | flops 5379850240 | bytes 17306624 | tf_op jit(solution)/shard_map/dot_general | solution.py:135
  134.4 77.2 %reduce-scatter.2.cloned.1.call-done = bf16[80,2048]{1,0:T(8,128)(2,1)} async-done(((bf16[1280,2048]{1,0:T(8,128)(2,1)}), bf16[80,2048]{1,0:T(8,128)(2,1)}) %reduce-scatter.2.cloned.1.call-update) | async-done | bytes 327696 | tf_op jit(solution)/shard_map/reduce_scatter | solution.py:139
  211.6 1.8 add_convert_fusion
  (31 shorter events, 0.2 us)
Async XLA Ops:
  6.5 117.4 %copy-start = (bf16[1,512,2048]{2,1,0:T(8,128)(2,1)S(1)}, bf16[1,512,2048]{2,1,0:T(8,128)(2,1)}, u32[]{:S(2)}) copy-start(bf16[1,512,2048]{2,1,0:T(8,128)(2,1)} %param.27) | copy-start | bytes 6291460
  6.5 33.8 %copy-start.7 = (bf16[512,512]{1,0:T(8,128)(2,1)S(1)}, bf16[512,512]{1,0:T(8,128)(2,1)}, u32[]{:S(2)}) copy-start(bf16[512,512]{1,0:T(8,128)(2,1)} %param.20) | copy-start | bytes 1572868
  6.5 33.8 %all-gather.4.cloned.1.call-start = ((), (), s32[]{:S(2)}) async-start(), calls=%async_computation.2 | async-start | bytes 1843200 | tf_op jit(solution)/shard_map/all_gather | solution.py:87
  12.9 29.6 %copy-start.3 = (bf16[160,512]{1,0:T(8,128)(2,1)S(1)}, bf16[160,512]{1,0:T(8,128)(2,1)}, u32[]{:S(2)}) copy-start(bf16[160,512]{1,0:T(8,128)(2,1)} %param.15) | copy-start | bytes 491524
  42.5 1.4 copy-start.1
  43.3 1.3 copy-start.8
  47.9 5.2 %copy-start.4 = (bf16[2048]{0:T(1024)(128)(2,1)S(1)}, bf16[2048]{0:T(1024)(128)(2,1)}, u32[]{:S(2)}) copy-start(bf16[2048]{0:T(1024)(128)(2,1)} %param.24) | copy-start | bytes 12292
  47.9 9.9 %copy-start.2 = (bf16[80,2048]{1,0:T(8,128)(2,1)S(1)}, bf16[80,2048]{1,0:T(8,128)(2,1)}, u32[]{:S(2)}) copy-start(bf16[80,2048]{1,0:T(8,128)(2,1)} %param.22) | copy-start | bytes 983044
  49.6 8.2 %all-to-all-start = ((bf16[2,80,512]{2,1,0:T(8,128)(2,1)}), bf16[2,80,512]{2,1,0:T(8,128)(2,1)S(1)}, u32[]{:S(2)}, u32[]{:S(2)}) async-start(bf16[2,80,512]{2,1,0:T(8,128)(2,1)} %bitcast.10), calls=%async_computation | async-start | bytes 327680 | tf_op jit(solution)/shard_map/all_to_all | solution.py:122
  53.0 63.3 %all-gather.6.cloned.1.call-start = ((), (), s32[]{:S(2)}) async-start(), calls=%async_computation.3 | async-start | bytes 5570560 | tf_op jit(solution)/shard_map/all_gather | solution.py:133
  57.8 4.2 %copy-start.5 = (f32[80,4]{0,1:T(4,128)S(1)}, f32[80,4]{0,1:T(4,128)}, u32[]{:S(2)}) copy-start(f32[80,4]{0,1:T(4,128)} %param.29) | copy-start | bytes 3844
  57.8 4.2 %copy-start.6 = (s32[80,4]{0,1:T(4,128)S(1)}, s32[80,4]{0,1:T(4,128)}, u32[]{:S(2)}) copy-start(s32[80,4]{0,1:T(4,128)} %param.28) | copy-start | bytes 3844
  61.9 149.7 %reduce-scatter.2.cloned.1.call-start = ((), (), s32[]{:S(2)}) async-start(), calls=%async_computation.4 | async-start | bytes 5570560 | tf_op jit(solution)/shard_map/reduce_scatter | solution.py:139
Sparse Core Ops, SparseCore 0:
  11.9 28.3 all-gather.3
  62.0 54.2 all-gather.5
  134.5 77.0 reduce-scatter.1
where the time goes:
time: 220 us
  waiting for transfers between devices  134 us (61%)
  blocking collectives  29.8 us (14%)
  matrix products  28.3 us (13%)
  between operations  13.4 us (6%)
  other arithmetic  8.51 us (4%)
  starting transfers between devices  3.51 us (2%)
  local copies, waits for them, and re-layouts  2.73 us (1%)
    reduce_scatter x1, waiting for transfers between devices, on_device(): lax.psum_scatter((own_share * product).astype(jnp.bfloat16), ('sp', 'tp')...  77.2 us
    all_gather x1, blocking collectives, on_device(): shares = lax.all_gather(share, ('sp', 'tp'), axis=0, tiled=True)  29.8 us
    all_gather x1, waiting for transfers between devices, on_device(): everyone = lax.all_gather(sent, 'sp', axis=0, tiled=True)  27.4 us
    all_gather x1, waiting for transfers between devices, on_device(): rows = lax.all_gather(normed, ('sp', 'tp'), axis=0, tiled=True)  24.3 us
    dot_general x1, matrix products, on_device(): jnp.dot(active, down_weight[0], preferred_element_type=jnp.float32)  10.5 us
    dot_general x1, matrix products, expert_active(): jnp.dot(rows, gate_w, preferred_element_type=jnp.float32)  7.56 us
    all_to_all x1, waiting for transfers between devices, on_device(): lax.all_to_all(attended.reshape(group, rows_dev, heads_dev * VALUE_WIDTH)...  4.68 us
  transfers between devices with their start and end apart: 4, of which 4 were waited for; matrix products, arithmetic and copies ran while one was open for 1% of the time, Pallas kernels for 0%

commit v1 on v0

--- a/solution.py
+++ b/solution.py
@@ -85,7 +85,6 @@
     latent_width = latent.shape[1]
     sent = jnp.concatenate([normed_latent, key_rot], axis=1)
     everyone = lax.all_gather(sent, "sp", axis=0, tiled=True)
-    shares = lax.all_gather(share, ("sp", "tp"), axis=0, tiled=True)
     all_latent = everyone[:, :latent_width]
     all_rot = everyone[:, latent_width:]
     keys = jnp.dot(all_latent, plain_key_matrix, preferred_element_type=jnp.float32).astype(
@@ -130,7 +129,11 @@
     projected = jnp.dot(own_rows, out_weight, preferred_element_type=jnp.float32)
     hidden = (residual.astype(jnp.float32) + projected).astype(jnp.bfloat16)
     normed = norm_scale(hidden, ffn_gain).astype(jnp.bfloat16)
-    rows = lax.all_gather(normed, ("sp", "tp"), axis=0, tiled=True)
+    shares, rows = jnp.split(
+        lax.all_gather(jnp.concatenate([share, normed], axis=1), ("sp", "tp"), axis=0, tiled=True),
+        [share.shape[1]],
+        axis=1,
+    )
     active = expert_active(rows, gate_weight[0], up_weight[0])
     product = jnp.dot(active, down_weight[0], preferred_element_type=jnp.float32)
     own_share = jnp.sum(

time: 220 us -> 260 us (1.18)
  waiting for transfers between devices: 134 us -> 198 us
  blocking collectives: 29.8 us -> 0 us
    all_gather x1, waiting for transfers between devices: 24.3 us -> 89.7 us  [on_device(): lax.all_gather(jnp.concatenate([share, normed], axis=1), ('sp', 'tp'), ax...]
    all_gather x1 -> x0, blocking collectives: 29.8 us -> none  [on_device(): shares = lax.all_gather(share, ('sp', 'tp'), axis=0, tiled=True)]
where the time goes in v1:
time: 260 us; the launch traced here: 259 us
  waiting for transfers between devices  198 us (76%)
  matrix products  30.8 us (12%)
  between operations  13.4 us (5%)
  other arithmetic  10.8 us (4%)
  starting transfers between devices  3.69 us (1%)
  local copies, waits for them, and re-layouts  2.72 us (1%)
    all_gather x1, waiting for transfers between devices, on_device(): lax.all_gather(jnp.concatenate([share, normed], axis=1), ('sp', 'tp'), ax...  89.7 us
    reduce_scatter x1, waiting for transfers between devices, on_device(): lax.psum_scatter((own_share * product).astype(jnp.bfloat16), ('sp', 'tp')...  76.8 us
    all_gather x1, waiting for transfers between devices, on_device(): everyone = lax.all_gather(sent, 'sp', axis=0, tiled=True)  26.7 us
    dot_general x1, matrix products, on_device(): jnp.dot(active, down_weight[0], preferred_element_type=jnp.float32)  11.3 us
    dot_general x1, matrix products, expert_active(): jnp.dot(rows, gate_w, preferred_element_type=jnp.float32)  9.21 us
  transfers between devices with their start and end apart: 4, of which 4 were waited for; matrix products, arithmetic and copies ran while one was open for 1% of the time, Pallas kernels for 0%

profile of v1, /device:TPU:0, one launch (start us, length us, event | category | flops | bytes accessed | tf_op | source)
XLA Modules:
  0.0 259.2 jit_solution(1321712183640586577)
XLA Ops:
  6.6 1.2 fusion.58
  7.8 0.7 convert_element_type.95
  8.5 0.8 convert_element_type.97
  9.2 0.2 multiply_cosine_fusion
  9.5 0.1 copy.43
  9.6 0.1 copy.42
  9.7 0.1 copy.44
  9.8 0.1 copy.45
  9.9 1.0 fusion.60
  11.0 0.8 concatenate.16
  11.8 0.0 all-gather.3.cloned.1.call-update
  11.8 0.7 convert_element_type.112
  12.5 1.0 copy.46
  13.6 26.7 %all-gather.3.cloned.1.call-done = bf16[1280,576]{1,0:T(8,128)(2,1)} async-done(((bf16[160,576]{1,0:T(8,128)(2,1)}), bf16[1280,576]{1,0:T(8,128)(2,1)}) %all-gather.3.cloned.1.call-update) | async-done | bytes 1474576 | tf_op jit(solution)/shard_map/all_gather | solution.py:87
  40.3 2.2 convolution_convert_fusion.1
  42.5 0.3 convolution_bitcast_fusion
  42.8 0.3 convolution_bitcast_fusion.1
  43.0 0.3 convolution_bitcast_fusion.2
  43.3 0.3 convolution_bitcast_fusion.3
  43.6 0.3 copy-done.1
  43.9 0.4 fusion.85
  44.3 0.3 fusion.47
  44.6 0.8 convolution_convert_fusion
  45.5 0.3 fusion.36
  45.8 0.4 fusion.86
  46.2 0.3 fusion.45
  46.5 0.3 fusion.35
  46.8 0.4 fusion.88
  47.2 0.3 fusion.41
  47.5 0.3 fusion.33
  47.9 0.4 fusion.87
  48.3 0.3 fusion.43
  48.6 0.3 fusion.34
  48.9 0.7 pad_maximum_fusion.1
  49.6 3.4 %all-to-all-start = ((bf16[2,80,512]{2,1,0:T(8,128)(2,1)}), bf16[2,80,512]{2,1,0:T(8,128)(2,1)S(1)}, u32[]{:S(2)}, u32[]{:S(2)}) async-start(bf16[2,80,512]{2,1,0:T(8,128)(2,1)} %bitcast.10), calls=%async_computation | async-start | bytes 327680 | tf_op jit(solution)/shard_map/all_to_all | solution.py:121
  53.0 0.0 all-gather.5.cloned.1.call-start
  53.1 0.1 copy.48
  53.2 4.6 %all-to-all-done = bf16[2,80,512]{2,1,0:T(8,128)(2,1)S(1)} async-done(((bf16[2,80,512]{2,1,0:T(8,128)(2,1)}), bf16[2,80,512]{2,1,0:T(8,128)(2,1)S(1)}, u32[]{:S(2)}, u32[]{:S(2)}) %all-to-all-start) | async-done | bytes 163872 | tf_op jit(solution)/shard_map/all_to_all | solution.py:121
  57.8 3.2 %multiply_reduce_fusion = (f32[80]{0:T(128)S(1)}, f32[80,2048]{1,0:T(8,128)S(1)}) fusion(bf16[80,1024]{1,0:T(8,128)(2,1)S(1)} %bitcast.49, bf16[1024,2048]{1,0:T(8,128)(2,1)} %param.23, bf16[80,2048]{1,0:T(8,128)(2,1)S(1)} %copy-done.2), kind=kOutput, calls=%fused_computation.58 | convolution fusion | flops 336527296 | bytes 5341504 | tf_op jit(solution)/shard_map/dot_general | solution.py:129
  61.0 0.1 fusion.61
  61.1 1.1 pad_maximum_fusion
  62.3 0.2 reduce-scatter.2.cloned.1.call-start
  62.5 89.7 %all-gather.5.cloned.1.call-done = f32[1280,2056]{1,0:T(8,128)} async-done(((f32[80,2056]{1,0:T(8,128)}), f32[1280,2056]{1,0:T(8,128)}) %all-gather.5.cloned.1.call-update) | async-done | bytes 10526736 | tf_op jit(solution)/shard_map/all_gather | solution.py:133
  152.2 1.3 fusion.49
  153.6 9.2 %fusion.7 = f32[1280,512]{1,0:T(8,128)} fusion(f32[1280,2056]{1,0:T(8,128)} %all-gather.5.cloned.1.call-done, bf16[1,2048,512]{2,1,0:T(8,128)(2,1)} %param.25), kind=kOutput, calls=%fused_computation.6 | convolution fusion | flops 2685009920 | bytes 9961472 | tf_op jit(solution)/shard_map/dot_general | solution.py:51
  162.8 11.3 %multiply_convert_fusion = bf16[1280,2048]{1,0:T(8,128)(2,1)} fusion(f32[1280]{0:T(1024)S(1)} %fusion.49, bf16[1,512,2048]{2,1,0:T(8,128)(2,1)S(1)} %copy-done, f32[1280,512]{1,0:T(8,128)} %fusion.7, f32[1280,2056]{1,0:T(8,128)} %all-gather.5.cloned.1.call-done, bf16[1,2048,512]{2,1,0:T(8,128)(2,1)} %param.26), kind=kOutput, calls=%fused_computation | convolution fusion | flops 5379850240 | bytes 17306624 | tf_op jit(solution)/shard_map/dot_general | solution.py:138
  174.1 76.8 %reduce-scatter.2.cloned.1.call-done = bf16[80,2048]{1,0:T(8,128)(2,1)} async-done(((bf16[1280,2048]{1,0:T(8,128)(2,1)}), bf16[80,2048]{1,0:T(8,128)(2,1)}) %reduce-scatter.2.cloned.1.call-update) | async-done | bytes 327696 | tf_op jit(solution)/shard_map/reduce_scatter | solution.py:142
  250.9 1.8 add_convert_fusion
  (28 shorter events, 0.2 us)
Async XLA Ops:
  6.5 156.2 %copy-start = (bf16[1,512,2048]{2,1,0:T(8,128)(2,1)S(1)}, bf16[1,512,2048]{2,1,0:T(8,128)(2,1)}, u32[]{:S(2)}) copy-start(bf16[1,512,2048]{2,1,0:T(8,128)(2,1)} %param.27) | copy-start | bytes 6291460
  6.5 33.8 %copy-start.6 = (bf16[512,512]{1,0:T(8,128)(2,1)S(1)}, bf16[512,512]{1,0:T(8,128)(2,1)}, u32[]{:S(2)}) copy-start(bf16[512,512]{1,0:T(8,128)(2,1)} %param.20) | copy-start | bytes 1572868
  6.5 33.8 %all-gather.3.cloned.1.call-start = ((), (), s32[]{:S(2)}) async-start(), calls=%async_computation.2 | async-start | bytes 1843200 | tf_op jit(solution)/shard_map/all_gather | solution.py:87
  13.6 28.9 %copy-start.3 = (bf16[160,512]{1,0:T(8,128)(2,1)S(1)}, bf16[160,512]{1,0:T(8,128)(2,1)}, u32[]{:S(2)}) copy-start(bf16[160,512]{1,0:T(8,128)(2,1)} %param.15) | copy-start | bytes 491524
  42.5 1.4 copy-start.1
  43.3 1.3 copy-start.7
  47.8 5.2 %copy-start.4 = (f32[80,4]{0,1:T(4,128)S(1)}, f32[80,4]{0,1:T(4,128)}, u32[]{:S(2)}) copy-start(f32[80,4]{0,1:T(4,128)} %param.29) | copy-start | bytes 3844
  47.9 5.2 %copy-start.5 = (s32[80,4]{0,1:T(4,128)S(1)}, s32[80,4]{0,1:T(4,128)}, u32[]{:S(2)}) copy-start(s32[80,4]{0,1:T(4,128)} %param.28) | copy-start | bytes 3844
  47.9 9.9 %copy-start.2 = (bf16[80,2048]{1,0:T(8,128)(2,1)S(1)}, bf16[80,2048]{1,0:T(8,128)(2,1)}, u32[]{:S(2)}) copy-start(bf16[80,2048]{1,0:T(8,128)(2,1)} %param.22) | copy-start | bytes 983044
  49.6 8.2 %all-to-all-start = ((bf16[2,80,512]{2,1,0:T(8,128)(2,1)}), bf16[2,80,512]{2,1,0:T(8,128)(2,1)S(1)}, u32[]{:S(2)}, u32[]{:S(2)}) async-start(bf16[2,80,512]{2,1,0:T(8,128)(2,1)} %bitcast.10), calls=%async_computation | async-start | bytes 327680 | tf_op jit(solution)/shard_map/all_to_all | solution.py:121
  53.0 99.2 %all-gather.5.cloned.1.call-start = ((), (), s32[]{:S(2)}) async-start(), calls=%async_computation.3 | async-start | bytes 11837440 | tf_op jit(solution)/shard_map/all_gather | solution.py:133
  62.3 188.6 %reduce-scatter.2.cloned.1.call-start = ((), (), s32[]{:S(2)}) async-start(), calls=%async_computation.4 | async-start | bytes 5570560 | tf_op jit(solution)/shard_map/reduce_scatter | solution.py:142
Sparse Core Ops, SparseCore 0:
  11.9 28.3 all-gather.2
  62.4 89.8 all-gather.4
  174.3 76.6 reduce-scatter.1
